TPU v7x, 32 devices: a whole 2x2x4 slice. The times are simulated.
32 devices in a mesh: fs: 16 (over z, y, x), tp: 2 (over core).
Axes of the slice: x: 2, y: 2, z: 4, core: 2. Of those that a mesh axis runs over, the one named last changes fastest.
Arguments:
- inputs: bfloat16 [6144, 2048], P('fs'), may hold values from -6 to 6
- gain: float32 [2048], replicated, may hold values from 0.1 to 1.9
- w_gate: bfloat16 [2048, 2816], P('fs', 'tp'), may hold values from -0.125 to 0.125
- w_up: bfloat16 [2048, 2816], P('fs', 'tp'), may hold values from -0.125 to 0.125
- w_down: bfloat16 [2816, 2048], P('tp', 'fs'), may hold values from -0.109375 to 0.109375
- cotangent: bfloat16 [6144, 2048], P('fs'), may hold values from -6 to 6
Outputs:
- input_gradient: bfloat16 [6144, 2048], P('fs')
- grad_down: float32 [2816, 2048], P('tp', 'fs')
All inputs are finite; a program needn't handle non-finite values.
Results may differ from a plain program's by a relative error of at most 0.014.
Values may be sent and summed in bfloat16 or wider, within the bound.
A program may use at most 64 MiB of HBM per device.

v0:
```python
import jax
import jax.numpy as jnp
from jax import lax
from jax.sharding import PartitionSpec as P

EPSILON = 1e-06
HALF_STEP = 0.5


def contract_last(left, right):
    return lax.dot_general(
        left, right, (((1,), (1,)), ((), ())), preferred_element_type=jnp.float32
    )


def shards(inputs, gain, w_gate, w_up, w_down, cotangent):
    value_entries = inputs.astype(jnp.float32)
    inverse_norm_factor = lax.rsqrt(
        jnp.mean(value_entries * value_entries, axis=-1, keepdims=True) + EPSILON
    )
    normalized_input = value_entries * inverse_norm_factor
    normalized_rows = (normalized_input * gain).astype(jnp.bfloat16)
    whole_gate, whole_up = (
        lax.all_gather(w_gate, "fs", axis=0, tiled=True),
        lax.all_gather(w_up, "fs", axis=0, tiled=True),
    )
    gate_value = jnp.dot(normalized_rows, whole_gate, preferred_element_type=jnp.float32)
    up_projection_value = jnp.dot(normalized_rows, whole_up, preferred_element_type=jnp.float32)
    sigmoid_gate = jax.nn.sigmoid(gate_value)
    hidden = (gate_value * sigmoid_gate * up_projection_value).astype(jnp.bfloat16)
    d_hidden = HALF_STEP * contract_last(
        cotangent, lax.all_gather(w_down, "fs", axis=1, tiled=True)
    )
    down_term = HALF_STEP * lax.dot_general(
        hidden, cotangent, (((0,), (0,)), ((), ())), preferred_element_type=jnp.float32
    )
    grad_down = lax.psum_scatter(down_term, "fs", scatter_dimension=1, tiled=True)
    d_gate = (
        d_hidden * up_projection_value * sigmoid_gate * (1.0 + gate_value * (1.0 - sigmoid_gate))
    ).astype(jnp.bfloat16)
    d_up = (d_hidden * gate_value * sigmoid_gate).astype(jnp.bfloat16)
    partial_term = contract_last(d_gate, whole_gate) + contract_last(d_up, whole_up)
    d_normed = lax.psum(partial_term.astype(jnp.bfloat16), "tp").astype(jnp.float32)
    scaled_hidden = d_normed * gain
    input_gradient = inverse_norm_factor * (
        scaled_hidden
        - normalized_input * jnp.mean(scaled_hidden * normalized_input, axis=-1, keepdims=True)
    )
    return (input_gradient.astype(jnp.bfloat16), grad_down)


def solution(mesh):
    in_specs = (P("fs", None), P(), P("fs", "tp"), P("fs", "tp"), P("tp", "fs"), P("fs", None))
    out_specs = (P("fs", None), P("tp", "fs"))
    return jax.shard_map(shards, mesh=mesh, in_specs=in_specs, out_specs=out_specs, check_vma=False)
```

profile of v0, /device:TPU:10, one launch (start us, length us, event | category | flops | bytes accessed | tf_op | source)
XLA Modules:
  0.0 587.9 jit_solution(5369307967862374800)
XLA Ops:
  7.2 0.0 copy-start
  7.2 0.0 copy-start.1
  7.2 0.0 copy-start.3
  7.2 0.0 all-gather.8.cloned.1.call-start
  7.2 0.7 all-gather.8.cloned.1.call-update
  7.9 0.0 all-gather.6.cloned.1.call-start
  8.0 0.7 all-gather.6.cloned.1.call-update
  8.7 0.0 all-gather.4.cloned.1.call-start
  8.7 0.7 all-gather.4.cloned.1.call-update
  9.4 0.0 all-reduce.2.cloned.1.call-start
  9.5 1.8 fusion.8
  11.3 89.2 %all-gather.8.cloned.1.call-done = bf16[2048,1408]{1,0:T(8,128)(2,1)} async-done(((bf16[128,1408]{1,0:T(8,128)(2,1)}), bf16[2048,1408]{1,0:T(8,128)(2,1)}) %all-gather.8.cloned.1.call-update) | async-done | bytes 5767184 | tf_op jit(solution)/shard_map/all_gather | solution.py:24
  100.5 0.0 copy-done.1
  100.5 0.0 copy-done.3
  100.5 6.6 %fusion.13 = f32[384,1408]{1,0:T(8,128)} fusion(bf16[2048,1408]{1,0:T(8,128)(2,1)} %all-gather.8.cloned.1.call-done, bf16[384,2048]{1,0:T(8,128)(2,1)S(1)} %copy-done.1, f32[2048]{0:T(1024)S(1)} %copy-done.3, f32[384]{0:T(512)S(1)} %add_rsqrt_fusion), kind=kOutput, calls=%fused_computation.23 | convolution fusion | flops 2217738240 | bytes 9512448 | tf_op jit(solution)/shard_map/dot_general | solution.py:27
  107.1 83.5 %all-gather.6.cloned.1.call-done = bf16[2048,1408]{1,0:T(8,128)(2,1)} async-done(((bf16[128,1408]{1,0:T(8,128)(2,1)}), bf16[2048,1408]{1,0:T(8,128)(2,1)}) %all-gather.6.cloned.1.call-update) | async-done | bytes 5767184 | tf_op jit(solution)/shard_map/all_gather | solution.py:25
  190.6 6.7 %fusion.15 = f32[384,1408]{1,0:T(8,128)} fusion(bf16[2048,1408]{1,0:T(8,128)(2,1)} %all-gather.6.cloned.1.call-done, bf16[384,2048]{1,0:T(8,128)(2,1)S(1)} %copy-done.1, f32[2048]{0:T(1024)S(1)} %copy-done.3, f32[384]{0:T(512)S(1)} %add_rsqrt_fusion), kind=kOutput, calls=%fused_computation.24 | convolution fusion | flops 2217738240 | bytes 9512448 | tf_op jit(solution)/shard_map/dot_general | solution.py:28
  197.3 100.4 %all-gather.4.cloned.1.call-done = bf16[1408,2048]{1,0:T(8,128)(2,1)} async-done(((bf16[1408,128]{1,0:T(8,128)(2,1)}), bf16[1408,2048]{1,0:T(8,128)(2,1)}) %all-gather.4.cloned.1.call-update) | async-done | bytes 5767184 | tf_op jit(solution)/shard_map/all_gather | solution.py:32
  297.7 0.0 copy-done
  297.7 0.0 copy-start.4
  297.7 0.0 copy-start.5
  297.7 0.0 copy-start.6
  297.7 0.0 slice-start
  297.7 5.4 convolution_multiply_fusion.1
  303.2 0.0 copy-done.4
  303.2 0.0 copy-done.5
  303.2 0.1 copy-done.6
  303.3 0.0 slice-start.1
  303.3 3.2 fusion.9
  306.5 0.0 slice-done
  306.5 0.0 slice-done.1
  306.6 3.8 add_convert_fusion
  310.4 0.0 all-reduce.2.cloned.1.call-update
  310.4 0.2 reduce-scatter.2.cloned.1.call-start
  310.6 8.5 %convolution_multiply_fusion = f32[1408,2048]{1,0:T(8,128)} fusion(bf16[384,2048]{1,0:T(8,128)(2,1)S(1)} %copy-done, f32[384,1408]{1,0:T(8,128)} %fusion.15, f32[384,1408]{1,0:T(8,128)} %fusion.13), kind=kOutput, calls=%fused_computation | convolution fusion | flops 2220720128 | bytes 17432576 | tf_op jit(solution)/shard_map/dot_general | solution.py:34
  319.1 0.0 reduce-scatter.2.cloned.1.call-update
  319.1 13.0 %all-reduce.2.cloned.1.call-done = bf16[384,2048]{1,0:T(8,128)(2,1)} async-done(((bf16[384,2048]{1,0:T(8,128)(2,1)}), bf16[384,2048]{1,0:T(8,128)(2,1)}) %all-reduce.2.cloned.1.call-update) | async-done | bytes 1572880 | tf_op jit(solution)/shard_map/psum | solution.py:43
  332.1 0.0 copy-start.2
  332.1 2.3 fusion.4
  334.4 0.0 copy-done.2
  334.4 2.0 fusion.7
  336.5 245.0 %reduce-scatter.2.cloned.1.call-done = f32[1408,128]{1,0:T(8,128)} async-done(((f32[1408,2048]{1,0:T(8,128)}), f32[1408,128]{1,0:T(8,128)}) %reduce-scatter.2.cloned.1.call-update) | async-done | bytes 720912 | tf_op jit(solution)/shard_map/reduce_scatter | solution.py:37
  (3 shorter events, 0.0 us)
Async XLA Ops:
  7.2 290.6 %copy-start = (bf16[384,2048]{1,0:T(8,128)(2,1)S(1)}, bf16[384,2048]{1,0:T(8,128)(2,1)}, u32[]{:S(2)}) copy-start(bf16[384,2048]{1,0:T(8,128)(2,1)} %param.11) | copy-start | bytes 4718596
  7.2 93.3 %copy-start.1 = (bf16[384,2048]{1,0:T(8,128)(2,1)S(1)}, bf16[384,2048]{1,0:T(8,128)(2,1)}, u32[]{:S(2)}) copy-start(bf16[384,2048]{1,0:T(8,128)(2,1)} %param.6) | copy-start | bytes 4718596
  7.2 93.3 %copy-start.3 = (f32[2048]{0:T(1024)S(1)}, f32[2048]{0:T(1024)}, u32[]{:S(2)}) copy-start(f32[2048]{0:T(1024)} %param.7) | copy-start | bytes 24580
  7.2 93.3 %all-gather.8.cloned.1.call-start = ((), (), s32[]{:S(2)}) async-start(), calls=%async_computation.3 | async-start | bytes 6127616 | tf_op jit(solution)/shard_map/all_gather | solution.py:24
  7.9 182.7 %all-gather.6.cloned.1.call-start = ((), (), s32[]{:S(2)}) async-start(), calls=%async_computation.2 | async-start | bytes 6127616 | tf_op jit(solution)/shard_map/all_gather | solution.py:25
  8.7 289.0 %all-gather.4.cloned.1.call-start = ((), (), s32[]{:S(2)}) async-start(), calls=%async_computation.1 | async-start | bytes 6127616 | tf_op jit(solution)/shard_map/all_gather | solution.py:32
  9.4 322.7 %all-reduce.2.cloned.1.call-start = ((), (), s32[]{:S(2)}) async-start(), calls=%async_computation.4 | async-start | bytes 3145728 | tf_op jit(solution)/shard_map/psum | solution.py:43
  297.7 5.4 copy-start.4
  297.7 5.5 copy-start.5
  297.7 5.6 copy-start.6
  297.7 8.8 %slice-start = ((s8[5767168]{0:T(1024)(128)(4,1)}), s8[4194304]{0:T(1024)(128)(4,1)S(1)}, s32[]{:S(2)}) async-start(s8[5767168]{0:T(1024)(128)(4,1)} %bitcast.7), calls=%async_computation.6 | async-start | bytes 8388608
  303.3 3.2 slice-start.1
  310.4 271.0 %reduce-scatter.2.cloned.1.call-start = ((), (), s32[]{:S(2)}) async-start(), calls=%async_computation.5 | async-start | bytes 12255232 | tf_op jit(solution)/shard_map/reduce_scatter | solution.py:37
  332.1 2.3 copy-start.2
Sparse Core Ops, SparseCore 0:
  10.7 89.7 all-gather.7
  103.2 87.4 all-gather.5
  193.3 104.3 all-gather.3
  310.5 21.5 all-reduce.1
  334.9 246.5 reduce-scatter.1
where the time goes:
time: 588 us
  waiting for transfers between devices  533 us (91%)
  matrix products  34.2 us (6%)
  between operations  13.9 us (2%)
  other arithmetic  6.11 us (1%)
    reduce_scatter x1, waiting for transfers between devices, shards(): lax.psum_scatter(down_term, 'fs', scatter_dimension=1, tiled=True)  245 us
    all_gather x1, waiting for transfers between devices, shards(): lax.all_gather(w_down, 'fs', axis=1, tiled=True)  100 us
    all_gather x1, waiting for transfers between devices, shards(): lax.all_gather(w_gate, 'fs', axis=0, tiled=True)  89.2 us
    all_gather x1, waiting for transfers between devices, shards(): lax.all_gather(w_up, 'fs', axis=0, tiled=True)  83.5 us
    psum x1, waiting for transfers between devices, shards(): lax.psum(partial_term.astype(jnp.bfloat16), 'tp').astype(jnp.float32)  13 us
    dot_general x3, matrix products, contract_last(): lax.dot_general(left, right, (((1,), (1,)), ((), ())), preferred_element_...  12.4 us
  transfers between devices with their start and end apart: 5, of which 5 were waited for; matrix products, arithmetic and copies ran while one was open for 5% of the time, Pallas kernels for 0%

commit v1 on v0

--- a/solution.py
+++ b/solution.py
@@ -29,7 +29,7 @@
     sigmoid_gate = jax.nn.sigmoid(gate_value)
     hidden = (gate_value * sigmoid_gate * up_projection_value).astype(jnp.bfloat16)
     d_hidden = HALF_STEP * contract_last(
-        cotangent, lax.all_gather(w_down, "fs", axis=1, tiled=True)
+        cotangent, jnp.concatenate(lax.all_gather(w_down, "fs"), axis=1)
     )
     down_term = HALF_STEP * lax.dot_general(
         hidden, cotangent, (((0,), (0,)), ((), ())), preferred_element_type=jnp.float32

time: 588 us -> 569 us (0.968)
  waiting for transfers between devices: 533 us -> 505 us
  local copies, waits for them, and re-layouts: 0.19 us -> 8.63 us
    all_gather x1, waiting for transfers between devices: 89.2 us -> 75 us  [shards(): lax.all_gather(w_gate, 'fs', axis=0, tiled=True)]
    all_gather x1, waiting for transfers between devices: 100 us -> 89.2 us  [shards(): lax.all_gather(w_down, 'fs')]
    reshape x0 -> x1, local copies, waits for them, and re-layouts: none -> 8.23 us  [shards(): jnp.concatenate(lax.all_gather(w_down, 'fs'), axis=1)]
  transfers between devices with their start and end apart: 5 -> 5, of which waited for: 5 -> 5; matrix products, arithmetic and copies ran while one was open for 5% -> 6% of each run, Pallas kernels for 0% -> 0%
where the time goes in v1:
time: 569 us
  waiting for transfers between devices  505 us (89%)
  matrix products  34.5 us (6%)
  between operations  13.8 us (2%)
  local copies, waits for them, and re-layouts  8.63 us (2%)
  other arithmetic  6.13 us (1%)
    reduce_scatter x1, waiting for transfers between devices, shards(): lax.psum_scatter(down_term, 'fs', scatter_dimension=1, tiled=True)  245 us
    all_gather x1, waiting for transfers between devices, shards(): lax.all_gather(w_down, 'fs')  89.2 us
    all_gather x1, waiting for transfers between devices, shards(): lax.all_gather(w_up, 'fs', axis=0, tiled=True)  83.4 us
    all_gather x1, waiting for transfers between devices, shards(): lax.all_gather(w_gate, 'fs', axis=0, tiled=True)  75 us
    dot_general x3, matrix products, contract_last(): lax.dot_general(left, right, (((1,), (1,)), ((), ())), preferred_element_...  13.9 us
  transfers between devices with their start and end apart: 5, of which 5 were waited for; matrix products, arithmetic and copies ran while one was open for 6% of the time, Pallas kernels for 0%

profile of v1, /device:TPU:10, one launch (start us, length us, event | category | flops | bytes accessed | tf_op | source)
XLA Modules:
  0.0 569.0 jit_solution(7624442295028113220)
XLA Ops:
  7.2 0.0 copy-start
  7.2 0.0 all-gather.9.cloned.1.call-start
  7.2 0.7 all-gather.9.cloned.1.call-update
  7.9 0.0 all-gather.7.cloned.1.call-start
  8.0 0.7 all-gather.7.cloned.1.call-update
  8.7 0.0 all-gather.5.cloned.1.call-start
  8.7 0.7 all-gather.5.cloned.1.call-update
  9.4 0.0 all-reduce.2.cloned.1.call-start
  9.4 1.8 fusion.8
  11.2 89.2 %all-gather.9.cloned.1.call-done = bf16[22528,128]{1,0:T(8,128)(2,1)} async-done(((bf16[1408,128]{1,0:T(8,128)(2,1)}), bf16[22528,128]{1,0:T(8,128)(2,1)}) %all-gather.9.cloned.1.call-update) | async-done | bytes 5767184 | tf_op jit(solution)/shard_map/all_gather | solution.py:32
  100.5 8.2 %copy.8 = bf16[1408,16,128]{0,2,1:T(8,128)(2,1)} copy(bf16[1408,16,128]{2,0,1:T(8,128)(2,1)} %bitcast.11) | data formatting | bytes 11534336 | tf_op jit(solution)/shard_map/reshape | solution.py:32
  108.7 0.0 copy-done
  108.7 0.0 copy-start.1
  108.7 0.0 copy-start.3
  108.7 6.9 %convolution_multiply_fusion.1 = f32[384,1408]{1,0:T(8,128)} fusion(bf16[384,2048]{1,0:T(8,128)(2,1)S(1)} %copy-done, bf16[1408,2048]{0,1:T(8,128)(2,1)} %bitcast.12), kind=kOutput, calls=%fused_computation.14 | convolution fusion | flops 2215133184 | bytes 9502720 | tf_op jit(solution)/shard_map/dot_general | solution.py:11
  115.6 75.0 %all-gather.7.cloned.1.call-done = bf16[2048,1408]{1,0:T(8,128)(2,1)} async-done(((bf16[128,1408]{1,0:T(8,128)(2,1)}), bf16[2048,1408]{1,0:T(8,128)(2,1)}) %all-gather.7.cloned.1.call-update) | async-done | bytes 5767184 | tf_op jit(solution)/shard_map/all_gather | solution.py:24
  190.6 0.0 copy-done.1
  190.6 0.0 copy-done.3
  190.6 6.8 %fusion.13 = f32[384,1408]{1,0:T(8,128)} fusion(bf16[2048,1408]{1,0:T(8,128)(2,1)} %all-gather.7.cloned.1.call-done, bf16[384,2048]{1,0:T(8,128)(2,1)S(1)} %copy-done.1, f32[2048]{0:T(1024)S(1)} %copy-done.3, f32[384]{0:T(512)S(1)} %add_rsqrt_fusion), kind=kOutput, calls=%fused_computation.23 | convolution fusion | flops 2217738240 | bytes 9512448 | tf_op jit(solution)/shard_map/dot_general | solution.py:27
  197.4 83.4 %all-gather.5.cloned.1.call-done = bf16[2048,1408]{1,0:T(8,128)(2,1)} async-done(((bf16[128,1408]{1,0:T(8,128)(2,1)}), bf16[2048,1408]{1,0:T(8,128)(2,1)}) %all-gather.5.cloned.1.call-update) | async-done | bytes 5767184 | tf_op jit(solution)/shard_map/all_gather | solution.py:25
  280.8 0.0 copy-start.4
  280.8 0.0 copy-start.6
  280.8 0.0 copy-start.8
  280.8 5.4 fusion.15
  286.2 0.0 copy-done.4
  286.2 0.0 copy-done.6
  286.2 0.1 copy-done.8
  286.4 0.0 copy-start.7
  286.4 0.0 copy-start.5
  286.4 3.2 fusion.9
  289.6 0.0 copy-done.7
  289.6 0.2 copy-done.5
  289.8 3.8 add_convert_fusion
  293.6 0.0 all-reduce.2.cloned.1.call-update
  293.6 0.2 reduce-scatter.2.cloned.1.call-start
  293.8 8.4 %convolution_multiply_fusion = f32[1408,2048]{1,0:T(8,128)} fusion(bf16[384,2048]{1,0:T(8,128)(2,1)S(1)} %copy-done, f32[384,1408]{1,0:T(8,128)} %copy-done.7, f32[384,1408]{1,0:T(8,128)} %fusion.13), kind=kOutput, calls=%fused_computation | convolution fusion | flops 2220720128 | bytes 17432576 | tf_op jit(solution)/shard_map/dot_general | solution.py:34
  302.3 0.0 reduce-scatter.2.cloned.1.call-update
  302.3 10.9 %all-reduce.2.cloned.1.call-done = bf16[384,2048]{1,0:T(8,128)(2,1)} async-done(((bf16[384,2048]{1,0:T(8,128)(2,1)}), bf16[384,2048]{1,0:T(8,128)(2,1)}) %all-reduce.2.cloned.1.call-update) | async-done | bytes 1572880 | tf_op jit(solution)/shard_map/psum | solution.py:43
  313.2 0.0 copy-start.2
  313.2 2.3 fusion.4
  315.5 0.0 copy-done.2
  315.5 2.0 fusion.7
  317.5 244.9 %reduce-scatter.2.cloned.1.call-done = f32[1408,128]{1,0:T(8,128)} async-done(((f32[1408,2048]{1,0:T(8,128)}), f32[1408,128]{1,0:T(8,128)}) %reduce-scatter.2.cloned.1.call-update) | async-done | bytes 720912 | tf_op jit(solution)/shard_map/reduce_scatter | solution.py:37
  (2 shorter events, 0.0 us)
Async XLA Ops:
  7.2 101.5 %copy-start = (bf16[384,2048]{1,0:T(8,128)(2,1)S(1)}, bf16[384,2048]{1,0:T(8,128)(2,1)}, u32[]{:S(2)}) copy-start(bf16[384,2048]{1,0:T(8,128)(2,1)} %param.11) | copy-start | bytes 4718596
  7.2 93.3 %all-gather.9.cloned.1.call-start = ((), (), s32[]{:S(2)}) async-start(), calls=%async_computation.5 | async-start | bytes 6127616 | tf_op jit(solution)/shard_map/all_gather | solution.py:32
  7.9 182.7 %all-gather.7.cloned.1.call-start = ((), (), s32[]{:S(2)}) async-start(), calls=%async_computation.2 | async-start | bytes 6127616 | tf_op jit(solution)/shard_map/all_gather | solution.py:24
  8.7 272.1 %all-gather.5.cloned.1.call-start = ((), (), s32[]{:S(2)}) async-start(), calls=%async_computation.1 | async-start | bytes 6127616 | tf_op jit(solution)/shard_map/all_gather | solution.py:25
  9.4 303.8 %all-reduce.2.cloned.1.call-start = ((), (), s32[]{:S(2)}) async-start(), calls=%async_computation.3 | async-start | bytes 3145728 | tf_op jit(solution)/shard_map/psum | solution.py:43
  108.7 81.9 %copy-start.1 = (bf16[384,2048]{1,0:T(8,128)(2,1)S(1)}, bf16[384,2048]{1,0:T(8,128)(2,1)}, u32[]{:S(2)}) copy-start(bf16[384,2048]{1,0:T(8,128)(2,1)} %param.6) | copy-start | bytes 4718596
  108.7 81.9 %copy-start.3 = (f32[2048]{0:T(1024)S(1)}, f32[2048]{0:T(1024)}, u32[]{:S(2)}) copy-start(f32[2048]{0:T(1024)} %param.7) | copy-start | bytes 24580
  280.8 5.5 copy-start.4
  280.8 5.5 copy-start.6
  280.8 5.6 copy-start.8
  286.4 3.2 copy-start.7
  286.4 3.4 copy-start.5
  293.6 268.9 %reduce-scatter.2.cloned.1.call-start = ((), (), s32[]{:S(2)}) async-start(), calls=%async_computation.4 | async-start | bytes 12255232 | tf_op jit(solution)/shard_map/reduce_scatter | solution.py:37
  313.2 2.3 copy-start.2
Sparse Core Ops, SparseCore 0:
  10.7 89.7 all-gather.8
  103.2 87.4 all-gather.6
  193.3 87.4 all-gather.4
  293.7 19.4 all-reduce.1
  315.9 246.5 reduce-scatter.1
